TPU v7x, 32 devices: a whole 2x2x4 slice. The times are simulated.
32 devices in a mesh: ep: 32 (over z, y, x, core).
Axes of the slice: x: 2, y: 2, z: 4, core: 2. Of those that a mesh axis runs over, the one named last changes fastest.
Arguments:
- tokens: bfloat16 [128, 2048], P('ep'), may hold values from -6 to 6
- norm_gain: float32 [2048], replicated, may hold values from 0.1 to 1.9
- routes: int32 [128, 2], P('ep'), may hold values from 0 to 1, all different within a row; in each aligned block of 4 rows (0 to 3, 4 to 7, ...) at most 4 rows name the same one
- route_weight: float32 [128, 2], P('ep'), may hold values from 0.1 to 1
- gate_weight: bfloat16 [2048, 14336], P(None, 'ep'), may hold values from -0.125 to 0.125
- up_weight: bfloat16 [2048, 14336], P(None, 'ep'), may hold values from -0.125 to 0.125
- down_weight: bfloat16 [14336, 2048], P('ep'), may hold values from -0.0625 to 0.0625
Outputs:
- mixed: bfloat16 [128, 2048], P('ep')
Inputs may be any that keep to these rules, and one draw needn't show every extreme that they name: `routes`: each row names two different experts of 0 to 1; among the rows of one device no expert is named by more than 4 rows, and in some device one expert is named by exactly 4.
All inputs are finite; a program needn't handle non-finite values.
Results may differ from a plain program's by a relative error of at most 0.0095.
Values may be sent and summed in bfloat16 or wider, within the bound.
A program may use at most 64 MiB of HBM per device.

v0:
```python
import jax
import jax.numpy as jnp
from jax import lax
from jax.sharding import PartitionSpec as P

GROUP = 16


epsilon = 1e-06


def expert_rows(rows, gate_part, up_part, down_part):
    gate = jnp.dot(rows, gate_part, preferred_element_type=jnp.float32)
    upper = jnp.dot(rows, up_part, preferred_element_type=jnp.float32)
    hidden = (jax.nn.silu(gate) * upper).astype(jnp.bfloat16)
    return jnp.dot(hidden, down_part, preferred_element_type=jnp.float32)


def normalize(tokens, norm_gain):
    values = tokens.astype(jnp.float32)
    scale = lax.rsqrt(jnp.mean(values * values, axis=-1, keepdims=True) + epsilon)
    return (values * scale * norm_gain).astype(jnp.bfloat16)


def on_device(tokens, norm_gain, routes, route_weight, gate_weight, up_weight, down_weight):
    normed = normalize(tokens, norm_gain)
    tok_count = tokens.shape[0]
    width = tokens.shape[1]
    devices = lax.axis_size("ep")
    experts = devices // GROUP
    most = min(tok_count, max(tok_count // 2, (2 * tok_count + experts - 1) // experts))
    expert_ids = lax.broadcasted_iota(jnp.int32, (1, experts), 1)
    pairs = 2 * tok_count
    flat_experts = routes.reshape(pairs)
    flat_weights = route_weight.reshape(pairs)
    onehot = (flat_experts[:, None] == expert_ids).astype(jnp.int32)
    earlier = jnp.cumsum(onehot, axis=0) - onehot
    slot = jnp.sum(earlier * onehot, axis=1)
    target = flat_experts * most + slot
    slot_ids = lax.broadcasted_iota(jnp.int32, (experts * most, pairs), 0)
    placed = (slot_ids == target[None, :]).astype(jnp.float32)
    pair_rows = lax.broadcasted_iota(jnp.int32, (pairs, tok_count), 0) // 2
    pair_cols = lax.broadcasted_iota(jnp.int32, (pairs, tok_count), 1)
    pair_token = (pair_rows == pair_cols).astype(jnp.float32)
    picker = jnp.dot(placed, pair_token, precision=lax.Precision.HIGHEST)
    outgoing = jnp.dot(
        picker.astype(jnp.bfloat16), normed, preferred_element_type=jnp.float32
    ).astype(jnp.bfloat16)
    outgoing = jnp.broadcast_to(
        outgoing.reshape(experts, 1, most, width), (experts, GROUP, most, width)
    )
    outgoing = outgoing.reshape(devices, most, width)
    received = lax.all_to_all(outgoing, "ep", split_axis=0, concat_axis=0, tiled=True)
    count = received.shape[1]
    flat = received.reshape(devices * count, width)
    result = expert_rows(flat, gate_weight, up_weight, down_weight).reshape(devices, count, width)
    back = lax.all_to_all(result, "ep", split_axis=0, concat_axis=0, tiled=True)
    summed = jnp.sum(back.reshape(experts, GROUP, most, width), axis=1).reshape(
        experts * most, width
    )
    weighted_pairs = pair_token.T * flat_weights[None, :]
    selector = jnp.dot(weighted_pairs, placed.T, precision=lax.Precision.HIGHEST)
    mixed = jnp.dot(selector, summed, precision=lax.Precision.HIGHEST)
    return mixed.astype(jnp.bfloat16)


def solution(mesh):
    return jax.shard_map(
        on_device,
        mesh=mesh,
        in_specs=(
            P("ep", None),
            P(),
            P("ep", None),
            P("ep", None),
            P(None, "ep"),
            P(None, "ep"),
            P("ep", None),
        ),
        out_specs=P("ep", None),
        check_vma=False,
    )
```

profile of v0, /device:TPU:0, one launch (start us, length us, event | category | flops | bytes accessed | tf_op | source)
XLA Modules:
  0.0 63.7 jit_solution(17756324787006354052)
XLA Ops:
  0.0 0.0 copy-start
  0.0 1.0 %fusion.8 = f32[4]{0:T(128)S(1)} fusion(bf16[4,2048]{1,0:T(4,128)(2,1)} %param.7), kind=kLoop, calls=%fused_computation.15 | loop fusion | flops 24572 | bytes 16400 | tf_op jit(solution)/shard_map/reduce_sum | solution.py:21
  1.0 0.8 %copy.13 = s32[4,2]{1,0:T(4,128)S(1)} copy(s32[4,2]{0,1:T(2,128)} %param.9) | data formatting | bytes 64 | tf_op args[2]
  1.8 0.1 reshape.39
  1.9 0.2 reduce_window_sum.11
  2.1 0.3 convolution_convert_fusion.2
  2.3 0.9 %convolution_convert_fusion = bf16[8,2048]{1,0:T(8,128)(2,1)S(1)} fusion(bf16[8,4]{0,1:T(4,128)(2,1)S(1)} %convolution_convert_fusion.2, bf16[4,2048]{1,0:T(4,128)(2,1)} %param.7, f32[2048]{0:T(1024)} %param.8, f32[4]{0:T(128)S(1)} %add_rsqrt_fusion), kind=kOutput, calls=%fused_computation | convolution fusion | flops 180224 | bytes 57424 | tf_op jit(solution)/shard_map/dot_general | solution.py:46
  3.3 0.2 broadcast_in_dim.5
  3.5 22.8 %all_to_all.10 = bf16[32,4,2048]{2,1,0:T(4,128)(2,1)S(1)} all-to-all(bf16[32,4,2048]{2,1,0:T(4,128)(2,1)S(1)} %bitcast.11), channel_id=1, replica_groups=mesh['ep'=32] {'ep'}, dimensions={0} | all-to-all | bytes 1048576 | tf_op jit(solution)/shard_map/all_to_all | solution.py:53
  26.3 0.1 reshape.41
  26.4 2.8 %fusion.29 = f32[128,448]{0,1:T(8,128)} fusion(bf16[128,2048]{1,0:T(8,128)(2,1)S(1)} %reshape.41, bf16[2048,448]{0,1:T(8,128)(2,1)} %param.11), kind=kOutput, calls=%fused_computation.47 | convolution fusion | flops 234881024 | bytes 2588672 | tf_op jit(solution)/shard_map/dot_general | solution.py:13
  29.2 0.0 copy-done
  29.2 3.0 %fusion.1 = f32[128,2048]{1,0:T(8,128)S(1)} fusion(bf16[448,2048]{1,0:T(8,128)(2,1)S(1)} %copy-done, bf16[128,2048]{1,0:T(8,128)(2,1)S(1)} %reshape.41, bf16[2048,448]{0,1:T(8,128)(2,1)} %param.12, f32[128,448]{0,1:T(8,128)} %fusion.29), kind=kOutput, calls=%fused_computation.4 | convolution fusion | flops 470106112 | bytes 5472256 | tf_op jit(solution)/shard_map/dot_general | solution.py:16
  32.3 0.0 copy-start.1
  32.3 1.3 %reshape.42 = f32[32,4,2048]{2,1,0:T(4,128)} reshape(f32[128,2048]{1,0:T(8,128)S(1)} %fusion.1) | data formatting | bytes 2097152 | tf_op jit(solution)/shard_map/reshape | solution.py:56
  33.6 3.0 %all-to-all-start.1 = ((f32[32,4,2048]{2,1,0:T(4,128)}), f32[32,4,2048]{2,1,0:T(4,128)S(1)}, u32[]{:S(2)}, u32[]{:S(2)}) async-start(f32[32,4,2048]{2,1,0:T(4,128)} %reshape.42), calls=%async_computation.1 | async-start | bytes 2097152 | tf_op jit(solution)/shard_map/all_to_all | solution.py:57
  36.6 0.0 copy-done.1
  36.6 0.1 copy.12
  36.7 0.1 mul.46
  36.8 0.1 fusion.14
  36.9 25.9 %all-to-all-done.1 = f32[32,4,2048]{2,1,0:T(4,128)S(1)} async-done(((f32[32,4,2048]{2,1,0:T(4,128)}), f32[32,4,2048]{2,1,0:T(4,128)S(1)}, u32[]{:S(2)}, u32[]{:S(2)}) %all-to-all-start.1) | async-done | bytes 1048608 | tf_op jit(solution)/shard_map/all_to_all | solution.py:57
  62.8 0.1 bitcast_reduce_fusion
  62.9 0.8 %convolution_convert_fusion.1 = bf16[4,2048]{1,0:T(4,128)(2,1)} fusion(f32[4,8]{1,0:T(4,128)S(1)} %fusion.14, f32[8,2048]{1,0:T(8,128)S(1)} %reshape.44), kind=kOutput, calls=%fused_computation.1 | convolution fusion | flops 794624 | bytes 82048 | tf_op jit(solution)/shard_map/dot_general | solution.py:63
  (8 shorter events, 0.1 us)
Async XLA Ops:
  0.0 29.2 %copy-start = (bf16[448,2048]{1,0:T(8,128)(2,1)S(1)}, bf16[448,2048]{1,0:T(8,128)(2,1)}, u32[]{:S(2)}) copy-start(bf16[448,2048]{1,0:T(8,128)(2,1)} %param.13) | copy-start | bytes 5505028
  32.3 4.3 %copy-start.1 = (f32[4,2]{0,1:T(2,128)S(1)}, f32[4,2]{0,1:T(2,128)}, u32[]{:S(2)}) copy-start(f32[4,2]{0,1:T(2,128)} %param.10) | copy-start | bytes 100
  33.6 29.2 %all-to-all-start.1 = ((f32[32,4,2048]{2,1,0:T(4,128)}), f32[32,4,2048]{2,1,0:T(4,128)S(1)}, u32[]{:S(2)}, u32[]{:S(2)}) async-start(f32[32,4,2048]{2,1,0:T(4,128)} %reshape.42), calls=%async_computation.1 | async-start | bytes 2097152 | tf_op jit(solution)/shard_map/all_to_all | solution.py:57
where the time goes:
time: 64.1 us; the launch traced here: 63.7 us
  waiting for transfers between devices  25.9 us (40%)
  blocking collectives  22.8 us (36%)
  matrix products  7.95 us (12%)
  starting transfers between devices  2.97 us (5%)
  local copies, waits for them, and re-layouts  2.74 us (4%)
  other arithmetic  1.33 us (2%)
    all_to_all x1, waiting for transfers between devices, on_device(): back = lax.all_to_all(result, 'ep', split_axis=0, concat_axis=0, tiled=True)  25.9 us
    all_to_all x1, blocking collectives, on_device(): lax.all_to_all(outgoing, 'ep', split_axis=0, concat_axis=0, tiled=True)  22.8 us
    dot_general x1, matrix products, expert_rows(): return jnp.dot(hidden, down_part, preferred_element_type=jnp.float32)  3.04 us
    all_to_all x1, starting transfers between devices, on_device(): back = lax.all_to_all(result, 'ep', split_axis=0, concat_axis=0, tiled=True)  2.97 us
    dot_general x1, matrix products, expert_rows(): gate = jnp.dot(rows, gate_part, preferred_element_type=jnp.float32)  2.82 us
    reshape x1, local copies, waits for them, and re-layouts, on_device(): expert_rows(flat, gate_weight, up_weight, down_weight)  1.29 us
  transfers between devices with their start and end apart: 1, of which 1 were waited for; matrix products, arithmetic and copies ran while one was open for 0% of the time, Pallas kernels for 0%

commit v1 on v0

--- a/solution.py
+++ b/solution.py
@@ -1,12 +1,186 @@
+import functools
+
 import jax
 import jax.numpy as jnp
 from jax import lax
+from jax.experimental import pallas as pl
+from jax.experimental.pallas import tpu as pltpu
 from jax.sharding import PartitionSpec as P
 
 GROUP = 16
+CORES = 2
+PIECES = 2
 
 
 epsilon = 1e-06
+MESH = pl.DeviceIdType.MESH
+
+
+def mixture_kernel(
+    chips, tok_ref, gain_ref, routes_ref, weight_ref, gate_hbm, up_hbm, down_hbm, out_ref,
+    gathered, gate_v, up_v, down_v, rows_v, mine_v, pair_out, pair_in, sums_out, sums_in,
+    load_sem, tok_send, tok_recv, fwd_send, fwd_recv, pair_send, pair_recv, sum_send, sum_recv,
+):
+    tok_count, width = tok_ref.shape
+    me = lax.axis_index("ep")
+    chip = me // CORES
+    core = me % CORES
+    partner = chip * CORES + (1 - core)
+    piece = width // PIECES
+    half = chips * tok_count
+
+    loads = [
+        pltpu.make_async_copy(src, dst, load_sem.at[i])
+        for i, (src, dst) in enumerate(((gate_hbm, gate_v), (up_hbm, up_v), (down_hbm, down_v)))
+    ]
+    for load in loads:
+        load.start()
+
+    barrier = pltpu.get_barrier_semaphore()
+    for k in range(1, chips):
+        pl.semaphore_signal(
+            barrier, inc=1, device_id=(((chip + k) % chips) * CORES + core,), device_id_type=MESH
+        )
+    pl.semaphore_signal(barrier, inc=1, device_id=(partner,), device_id_type=MESH)
+
+    values = tok_ref[...].astype(jnp.float32)
+    scale = lax.rsqrt(jnp.mean(values * values, axis=-1, keepdims=True) + epsilon)
+    gathered[0, chip] = (values * scale * gain_ref[...]).astype(jnp.bfloat16)
+    pl.semaphore_wait(barrier, chips)
+
+    def to_partner(src, dst, send, recv):
+        return pltpu.make_async_remote_copy(
+            src_ref=src, dst_ref=dst, send_sem=send, recv_sem=recv,
+            device_id=(partner,), device_id_type=MESH,
+        )
+
+    spread = []
+    for k in range(1, chips):
+        copy = pltpu.make_async_remote_copy(
+            src_ref=gathered.at[0, chip], dst_ref=gathered.at[0, chip],
+            send_sem=tok_send.at[k], recv_sem=tok_recv.at[k],
+            device_id=(((chip + k) % chips) * CORES + core,), device_id_type=MESH,
+        )
+        copy.start()
+        spread.append(copy)
+    forward = []
+    copy = to_partner(gathered.at[0, chip], gathered.at[1, chip], fwd_send.at[0], fwd_recv.at[0])
+    copy.start()
+    forward.append(copy)
+    for k in range(1, chips):
+        spread[k - 1].wait_recv()
+        origin = (chip + chips - k) % chips
+        copy = to_partner(
+            gathered.at[0, origin], gathered.at[1, origin], fwd_send.at[k], fwd_recv.at[k]
+        )
+        copy.start()
+        forward.append(copy)
+
+    def lay_out(color):
+        block = gathered[color].astype(jnp.float32).reshape(half, width)
+        rows_v[color * half:(color + 1) * half, :] = block.astype(jnp.bfloat16)
+
+    lay_out(0)
+    for copy in forward:
+        copy.wait_recv()
+    lay_out(1)
+
+    rows = rows_v[...]
+    loads[0].wait()
+    gate = jnp.dot(rows, gate_v[...], preferred_element_type=jnp.float32)
+    loads[1].wait()
+    upper = jnp.dot(rows, up_v[...], preferred_element_type=jnp.float32)
+    hidden = (jax.nn.silu(gate) * upper).astype(jnp.bfloat16)
+    loads[2].wait()
+
+    pairs = []
+    for c in range(PIECES):
+        part = jnp.dot(
+            hidden, down_v[:, c * piece:(c + 1) * piece], preferred_element_type=jnp.float32
+        )
+        mine_v[c] = part[:half]
+        pair_out[c] = part[half:].astype(jnp.bfloat16)
+        copy = to_partner(pair_out.at[c], pair_in.at[c], pair_send.at[c], pair_recv.at[c])
+        copy.start()
+        pairs.append(copy)
+
+    results = []
+    for c in range(PIECES):
+        pairs[c].wait_recv()
+        total = mine_v[c] + pair_in[c].astype(jnp.float32)
+        sums_out[c] = total.reshape(chips, tok_count, piece).astype(jnp.bfloat16)
+        for k in range(1, chips):
+            target = (chip + k) % chips
+            copy = pltpu.make_async_remote_copy(
+                src_ref=sums_out.at[c, target], dst_ref=sums_in.at[c, chip],
+                send_sem=sum_send.at[c, k], recv_sem=sum_recv.at[c, k],
+                device_id=(target * CORES + core,), device_id_type=MESH,
+            )
+            copy.start()
+            results.append(copy)
+        sums_in[c, chip] = sums_out[c, chip]
+
+    experts = chips * CORES // GROUP
+    per_expert = chips // experts
+    routes = routes_ref[...]
+    weights = weight_ref[...]
+    shares = [
+        jnp.sum(jnp.where(routes == e, weights, 0.0), axis=1, keepdims=True)
+        for e in range(experts)
+    ]
+    for c in range(PIECES):
+        for copy in results[c * (chips - 1):(c + 1) * (chips - 1)]:
+            copy.wait_recv()
+        mixed = jnp.zeros((tok_count, piece), jnp.float32)
+        for e in range(experts):
+            block = sums_in[c, e * per_expert:(e + 1) * per_expert].astype(jnp.float32)
+            mixed = mixed + shares[e] * jnp.sum(block, axis=0)
+        out_ref[:, c * piece:(c + 1) * piece] = mixed.astype(jnp.bfloat16)
+
+    for copy in spread + forward + pairs + results:
+        copy.wait_send()
+
+
+def dense_on_device(tokens, norm_gain, routes, route_weight, gate_weight, up_weight, down_weight):
+    tok_count, width = tokens.shape
+    chips = lax.axis_size("ep") // CORES
+    hidden = gate_weight.shape[1]
+    vmem = pl.BlockSpec(memory_space=pltpu.VMEM)
+    anywhere = pl.BlockSpec(memory_space=pl.ANY)
+    half = chips * tok_count
+    piece = width // PIECES
+    dma = pltpu.SemaphoreType.DMA
+    return pl.pallas_call(
+        functools.partial(mixture_kernel, chips),
+        out_shape=jax.ShapeDtypeStruct((tok_count, width), jnp.bfloat16),
+        in_specs=[vmem] * 4 + [anywhere] * 3,
+        out_specs=vmem,
+        scratch_shapes=[
+            pltpu.VMEM((CORES, chips, tok_count, width), jnp.bfloat16),
+            pltpu.VMEM((width, hidden), jnp.bfloat16),
+            pltpu.VMEM((width, hidden), jnp.bfloat16),
+            pltpu.VMEM((hidden, width), jnp.bfloat16),
+            pltpu.VMEM((CORES * half, width), jnp.bfloat16),
+            pltpu.VMEM((PIECES, half, piece), jnp.float32),
+            pltpu.VMEM((PIECES, half, piece), jnp.bfloat16),
+            pltpu.VMEM((PIECES, half, piece), jnp.bfloat16),
+            pltpu.VMEM((PIECES, chips, tok_count, piece), jnp.bfloat16),
+            pltpu.VMEM((PIECES, chips, tok_count, piece), jnp.bfloat16),
+            dma((3,)),
+            dma((chips,)),
+            dma((chips,)),
+            dma((chips,)),
+            dma((chips,)),
+            dma((PIECES,)),
+            dma((PIECES,)),
+            dma((PIECES, chips)),
+            dma((PIECES, chips)),
+        ],
+        compiler_params=pltpu.CompilerParams(collective_id=0, has_side_effects=True),
+    )(
+        tokens, norm_gain.reshape(1, width), routes, route_weight,
+        gate_weight, up_weight, down_weight,
+    )
 
 
 def expert_rows(rows, gate_part, up_part, down_part):
@@ -65,8 +239,9 @@
 
 
 def solution(mesh):
+    every_expert = mesh.shape["ep"] == 2 * GROUP
     return jax.shard_map(
-        on_device,
+        dense_on_device if every_expert else on_device,
         mesh=mesh,
         in_specs=(
             P("ep", None),

time: 64.1 us -> 38.2 us (0.60)
  Pallas kernels: 0 us -> 27.4 us
  waiting for transfers between devices: 25.9 us -> 0 us
  blocking collectives: 22.8 us -> 0 us
  matrix products: 7.95 us -> 0 us
  local copies, waits for them, and re-layouts: 2.74 us -> 10.4 us
  starting transfers between devices: 2.97 us -> 0 us
  other arithmetic: 1.33 us -> 0 us
    pallas_call x0 -> x1, Pallas kernels: none -> 27.4 us  [dense_on_device(): pl.pallas_call(functools.partial(mixture_kernel, chips), out_shape=jax.Sh...]
    all_to_all x1 -> x0, waiting for transfers between devices: 25.9 us -> none  [on_device(): back = lax.all_to_all(result, 'ep', split_axis=0, concat_axis=0, tiled=True)]
    all_to_all x1 -> x0, blocking collectives: 22.8 us -> none  [on_device(): lax.all_to_all(outgoing, 'ep', split_axis=0, concat_axis=0, tiled=True)]
    unnamed x6 -> x7, local copies, waits for them, and re-layouts: 0.87 us -> 10.4 us
    dot_general x6 -> x0, matrix products: 7.95 us -> none  [the longest x1 3.04 us: expert_rows(): return jnp.dot(hidden, down_part, preferred_element_type=jnp.float32)]
    all_to_all x1 -> x0, starting transfers between devices: 2.97 us -> none  [on_device(): back = lax.all_to_all(result, 'ep', split_axis=0, concat_axis=0, tiled=True)]
    reshape x4 -> x0, local copies, waits for them, and re-layouts: 1.53 us -> none  [the longest x1 1.29 us: on_device(): expert_rows(flat, gate_weight, up_weight, down_weight)]
    reduce_sum x3 -> x0, other arithmetic: 1.12 us -> none  [the longest x1 0.98 us: normalize(): jnp.mean(values * values, axis=-1, keepdims=True) + epsilon]
  transfers between devices with their start and end apart: 1 -> 0, of which waited for: 1 -> 0; matrix products, arithmetic and copies ran while one was open for 0% -> 0% of each run, Pallas kernels for 0% -> 0%
where the time goes in v1:
time: 38.2 us; the launch traced here: 37.9 us
  Pallas kernels  27.4 us (72%)
  local copies, waits for them, and re-layouts  10.4 us (27%)
    pallas_call x1, Pallas kernels, dense_on_device(): pl.pallas_call(functools.partial(mixture_kernel, chips), out_shape=jax.Sh...  27.4 us
    unnamed x7, local copies, waits for them, and re-layouts  10.4 us

profile of v1, /device:TPU:0, one launch (start us, length us, event | category | flops | bytes accessed | tf_op | source)
XLA Modules:
  0.0 37.9 jit_solution(17630338968762111943)
XLA Ops:
  0.0 1.3 %copy.8.routes_ref = s32[4,2]{1,0:T(4,128)} copy(s32[4,2]{0,1:T(2,128)} %param.9) | data formatting | bytes 64 | tf_op args[2]
  1.3 1.3 %copy.9.weight_ref = f32[4,2]{1,0:T(4,128)} copy(f32[4,2]{0,1:T(2,128)} %param.10) | data formatting | bytes 64 | tf_op args[3]
  2.7 0.0 copy-start
  2.7 4.0 %copy.10.gate_hbm = bf16[2048,448]{1,0:T(8,128)(2,1)} copy(bf16[2048,448]{0,1:T(8,128)(2,1)} %param.11) | data formatting | bytes 3670016 | tf_op args[4]
  6.6 0.0 copy-done
  6.6 2.5 %copy.11.up_hbm = bf16[2048,448]{1,0:T(8,128)(2,1)} copy(bf16[2048,448]{0,1:T(8,128)(2,1)S(1)} %copy-done) | data formatting | bytes 3670016 | tf_op args[5]
  9.1 27.4 %shard_map.73 = bf16[4,2048]{1,0:T(4,128)(2,1)} custom-call(bf16[4,2048]{1,0:T(4,128)(2,1)} %tok_ref.1, f32[1,2048]{1,0:T(1,128)} %bitcast.1, s32[4,2]{1,0:T(4,128)} %copy.8.routes_ref, f32[4,2]{1,0:T(4,128)} %copy.9.weight_ref, bf16[2048,448]{1,0:T(8,128)(2,1)} %copy.10.gate_hbm, bf16[2048,448]{1,0:T(8,128)(2,1)} %copy.11.up_hbm, bf16[448,2048]{1,0:T(8,128)(2,1)} %down_hbm.1), custom_call_target="tpu_custom_call" | custom-call | tf_op jit(solution)/shard_map/pallas_call | solution.py:153
  36.5 1.3 %copy.13 = bf16[4,2048]{1,0:T(4,128)(2,1)} copy(bf16[4,2048]{1,0:T(4,128)(2,1)} %shard_map.73) | data formatting | bytes 32768
Async XLA Ops:
  2.7 4.0 %copy-start = (bf16[2048,448]{0,1:T(8,128)(2,1)S(1)}, bf16[2048,448]{0,1:T(8,128)(2,1)}, u32[]{:S(2)}) copy-start(bf16[2048,448]{0,1:T(8,128)(2,1)} %param.12) | copy-start | bytes 5505028

commit v2 on v1

--- a/solution.py
+++ b/solution.py
@@ -9,19 +9,25 @@
 
 GROUP = 16
 CORES = 2
-PIECES = 2
+PIECES = 1
 
 
 epsilon = 1e-06
 MESH = pl.DeviceIdType.MESH
 
 
+def times_transposed(rows, part):
+    return lax.dot_general(
+        rows, part, (((1,), (1,)), ((), ())), preferred_element_type=jnp.float32
+    )
+
+
 def mixture_kernel(
-    chips, tok_ref, gain_ref, routes_ref, weight_ref, gate_hbm, up_hbm, down_hbm, out_ref,
-    gathered, gate_v, up_v, down_v, rows_v, mine_v, pair_out, pair_in, sums_out, sums_in,
-    load_sem, tok_send, tok_recv, fwd_send, fwd_recv, pair_send, pair_recv, sum_send, sum_recv,
+    chips, tok_hbm, gain_hbm, routes_hbm, weight_hbm, gate_hbm, up_hbm, down_hbm, out_ref,
+    tok_ref, gain_ref, routes_ref, weight_ref, gathered, gate_v, up_v, down_v, rows_v, mine_v, pair_out, pair_in, sums_out, sums_in,
+    load_sem, small_sem, tok_send, tok_recv, fwd_send, fwd_recv, pair_send, pair_recv, sum_send, sum_recv,
 ):
-    tok_count, width = tok_ref.shape
+    tok_count, width = tok_hbm.shape
     me = lax.axis_index("ep")
     chip = me // CORES
     core = me % CORES
@@ -29,19 +35,33 @@
     piece = width // PIECES
     half = chips * tok_count
 
+    others = [(chip + k) % chips for k in range(1, chips)]
+
+    def twin(other):
+        return (other * CORES + core,)
+
+    small = [
+        pltpu.make_async_copy(src, dst, small_sem.at[i])
+        for i, (src, dst) in enumerate((
+            (tok_hbm, tok_ref), (gain_hbm, gain_ref),
+            (routes_hbm, routes_ref), (weight_hbm, weight_ref),
+        ))
+    ]
+    for load in small:
+        load.start()
     loads = [
         pltpu.make_async_copy(src, dst, load_sem.at[i])
         for i, (src, dst) in enumerate(((gate_hbm, gate_v), (up_hbm, up_v), (down_hbm, down_v)))
     ]
+    barrier = pltpu.get_barrier_semaphore()
+    for other in others:
+        pl.semaphore_signal(barrier, inc=1, device_id=twin(other), device_id_type=MESH)
+    pl.semaphore_signal(barrier, inc=1, device_id=(partner,), device_id_type=MESH)
+
     for load in loads:
         load.start()
-
-    barrier = pltpu.get_barrier_semaphore()
-    for k in range(1, chips):
-        pl.semaphore_signal(
-            barrier, inc=1, device_id=(((chip + k) % chips) * CORES + core,), device_id_type=MESH
-        )
-    pl.semaphore_signal(barrier, inc=1, device_id=(partner,), device_id_type=MESH)
+    for load in small:
+        load.wait()
 
     values = tok_ref[...].astype(jnp.float32)
     scale = lax.rsqrt(jnp.mean(values * values, axis=-1, keepdims=True) + epsilon)
@@ -55,23 +75,28 @@
         )
 
     spread = []
-    for k in range(1, chips):
+    for other in others:
         copy = pltpu.make_async_remote_copy(
             src_ref=gathered.at[0, chip], dst_ref=gathered.at[0, chip],
-            send_sem=tok_send.at[k], recv_sem=tok_recv.at[k],
-            device_id=(((chip + k) % chips) * CORES + core,), device_id_type=MESH,
+            send_sem=tok_send.at[other], recv_sem=tok_recv.at[chip],
+            device_id=twin(other), device_id_type=MESH,
         )
         copy.start()
         spread.append(copy)
     forward = []
-    copy = to_partner(gathered.at[0, chip], gathered.at[1, chip], fwd_send.at[0], fwd_recv.at[0])
+    copy = to_partner(
+        gathered.at[0, chip], gathered.at[1, chip], fwd_send.at[chip], fwd_recv.at[chip]
+    )
     copy.start()
     forward.append(copy)
-    for k in range(1, chips):
-        spread[k - 1].wait_recv()
-        origin = (chip + chips - k) % chips
+    for other in others[::-1]:
+        pltpu.make_async_remote_copy(
+            src_ref=gathered.at[0, other], dst_ref=gathered.at[0, other],
+            send_sem=tok_send.at[other], recv_sem=tok_recv.at[other],
+            device_id=twin(other), device_id_type=MESH,
+        ).wait_recv()
         copy = to_partner(
-            gathered.at[0, origin], gathered.at[1, origin], fwd_send.at[k], fwd_recv.at[k]
+            gathered.at[0, other], gathered.at[1, other], fwd_send.at[other], fwd_recv.at[other]
         )
         copy.start()
         forward.append(copy)
@@ -87,9 +112,9 @@
 
     rows = rows_v[...]
     loads[0].wait()
-    gate = jnp.dot(rows, gate_v[...], preferred_element_type=jnp.float32)
+    gate = times_transposed(rows, gate_v[...])
     loads[1].wait()
-    upper = jnp.dot(rows, up_v[...], preferred_element_type=jnp.float32)
+    upper = times_transposed(rows, up_v[...])
     hidden = (jax.nn.silu(gate) * upper).astype(jnp.bfloat16)
     loads[2].wait()
 
@@ -109,12 +134,11 @@
         pairs[c].wait_recv()
         total = mine_v[c] + pair_in[c].astype(jnp.float32)
         sums_out[c] = total.reshape(chips, tok_count, piece).astype(jnp.bfloat16)
-        for k in range(1, chips):
-            target = (chip + k) % chips
+        for other in others:
             copy = pltpu.make_async_remote_copy(
-                src_ref=sums_out.at[c, target], dst_ref=sums_in.at[c, chip],
-                send_sem=sum_send.at[c, k], recv_sem=sum_recv.at[c, k],
-                device_id=(target * CORES + core,), device_id_type=MESH,
+                src_ref=sums_out.at[c, other], dst_ref=sums_in.at[c, chip],
+                send_sem=sum_send.at[c, other], recv_sem=sum_recv.at[c, chip],
+                device_id=twin(other), device_id_type=MESH,
             )
             copy.start()
             results.append(copy)
@@ -125,12 +149,16 @@
     routes = routes_ref[...]
     weights = weight_ref[...]
     shares = [
-        jnp.sum(jnp.where(routes == e, weights, 0.0), axis=1, keepdims=True)
+        jnp.sum(jnp.where(routes == e, weights, 0.0), axis=0, keepdims=True).T
         for e in range(experts)
     ]
     for c in range(PIECES):
-        for copy in results[c * (chips - 1):(c + 1) * (chips - 1)]:
-            copy.wait_recv()
+        for other in others[::-1]:
+            pltpu.make_async_remote_copy(
+                src_ref=sums_out.at[c, other], dst_ref=sums_in.at[c, other],
+                send_sem=sum_send.at[c, other], recv_sem=sum_recv.at[c, other],
+                device_id=twin(other), device_id_type=MESH,
+            ).wait_recv()
         mixed = jnp.zeros((tok_count, piece), jnp.float32)
         for e in range(experts):
             block = sums_in[c, e * per_expert:(e + 1) * per_expert].astype(jnp.float32)
@@ -152,13 +180,17 @@
     dma = pltpu.SemaphoreType.DMA
     return pl.pallas_call(
         functools.partial(mixture_kernel, chips),
-        out_shape=jax.ShapeDtypeStruct((tok_count, width), jnp.bfloat16),
-        in_specs=[vmem] * 4 + [anywhere] * 3,
+        out_shape=pltpu.VMEM((tok_count, width), jnp.bfloat16),
+        in_specs=[anywhere] * 7,
         out_specs=vmem,
         scratch_shapes=[
+            pltpu.VMEM((tok_count, width), jnp.bfloat16),
+            pltpu.VMEM((1, width), jnp.float32),
+            pltpu.VMEM((2, tok_count), jnp.int32),
+            pltpu.VMEM((2, tok_count), jnp.float32),
             pltpu.VMEM((CORES, chips, tok_count, width), jnp.bfloat16),
-            pltpu.VMEM((width, hidden), jnp.bfloat16),
-            pltpu.VMEM((width, hidden), jnp.bfloat16),
+            pltpu.VMEM((hidden, width), jnp.bfloat16),
+            pltpu.VMEM((hidden, width), jnp.bfloat16),
             pltpu.VMEM((hidden, width), jnp.bfloat16),
             pltpu.VMEM((CORES * half, width), jnp.bfloat16),
             pltpu.VMEM((PIECES, half, piece), jnp.float32),
@@ -167,6 +199,7 @@
             pltpu.VMEM((PIECES, chips, tok_count, piece), jnp.bfloat16),
             pltpu.VMEM((PIECES, chips, tok_count, piece), jnp.bfloat16),
             dma((3,)),
+            dma((4,)),
             dma((chips,)),
             dma((chips,)),
             dma((chips,)),
@@ -178,8 +211,8 @@
         ],
         compiler_params=pltpu.CompilerParams(collective_id=0, has_side_effects=True),
     )(
-        tokens, norm_gain.reshape(1, width), routes, route_weight,
-        gate_weight, up_weight, down_weight,
+        tokens, norm_gain.reshape(1, width), routes.T, route_weight.T,
+        gate_weight.T, up_weight.T, down_weight,
     )
 
 

time: 38.2 us -> 26.1 us (0.68)
  local copies, waits for them, and re-layouts: 10.4 us -> 0.61 us
  Pallas kernels: 27.4 us -> 25.2 us
    unnamed x7 -> x1, local copies, waits for them, and re-layouts: 10.4 us -> 0.61 us
    pallas_call x1, Pallas kernels: 27.4 us -> 25.2 us  [dense_on_device(): pl.pallas_call(functools.partial(mixture_kernel, chips), out_shape=pltpu....]
where the time goes in v2:
time: 26.1 us; the launch traced here: 25.8 us
  Pallas kernels  25.2 us (97%)
  local copies, waits for them, and re-layouts  0.61 us (2%)
    pallas_call x1, Pallas kernels, dense_on_device(): pl.pallas_call(functools.partial(mixture_kernel, chips), out_shape=pltpu....  25.2 us
    unnamed x1, local copies, waits for them, and re-layouts  0.61 us

profile of v2, /device:TPU:0, one launch (start us, length us, event | category | flops | bytes accessed | tf_op | source)
XLA Modules:
  0.0 25.8 jit_solution(2159722298588032224)
XLA Ops:
  0.0 25.2 %shard_map.73 = bf16[4,2048]{1,0:T(4,128)(2,1)S(1)} custom-call(bf16[4,2048]{1,0:T(4,128)(2,1)} %tok_hbm.1, f32[1,2048]{1,0:T(1,128)} %bitcast.7, s32[2,4]{1,0:T(2,128)} %bitcast.8, f32[2,4]{1,0:T(2,128)} %bitcast.9, bf16[448,2048]{1,0:T(8,128)(2,1)} %bitcast.5, bf16[448,2048]{1,0:T(8,128)(2,1)} %bitcast.6, bf16[448,2048]{1,0:T(8,128)(2,1)} %down_hbm.1), custom_call_target="tpu_custom_call" | custom-call | tf_op jit(solution)/shard_map/pallas_call | solution.py:181
  25.2 0.6 %copy.9 = bf16[4,2048]{1,0:T(4,128)(2,1)} copy(bf16[4,2048]{1,0:T(4,128)(2,1)S(1)} %shard_map.73) | data formatting | bytes 32768
